TPU v7x, 32 devices: a whole 2x2x4 slice. The times are simulated.
32 devices in a mesh: grp: 2 (over x), sp: 4 (over y, core), tp: 4 (over z).
Axes of the slice: x: 2, y: 2, z: 4, core: 2. Of those that a mesh axis runs over, the one named last changes fastest.
Arguments:
- tokens: bfloat16 [8, 1024, 2048], P(('grp', 'tp'), 'sp'), parts along dimension 0, may hold values from -6 to 6
- kv_down: bfloat16 [2048, 512], replicated, may hold values from -0.125 to 0.125
- rope_down: bfloat16 [2048, 64], replicated, may hold values from -0.125 to 0.125
- kv_gain: float32 [512], replicated, may hold values from 0.1 to 1.9
- key_up: bfloat16 [512, 16, 128], replicated, may hold values from -0.25 to 0.25
- value_up: bfloat16 [512, 16, 128], replicated, may hold values from -0.25 to 0.25
- query_nope: bfloat16 [8, 16, 128], P(('grp', 'sp'), 'tp'), parts along dimension 0, may hold values from -180 to 180
- query_rope: bfloat16 [8, 16, 64], P(('grp', 'sp'), 'tp'), parts along dimension 0, may hold values from -180 to 180
Outputs:
- key_cache: bfloat16 [8, 16, 1024, 128], P(('grp', 'sp'), 'tp'), parts along dimension 0
- value_cache: bfloat16 [8, 16, 1024, 128], P(('grp', 'sp'), 'tp'), parts along dimension 0
- rope_cache: bfloat16 [8, 1024, 64], P(('grp', 'sp')), parts along dimension 0
- read_out: bfloat16 [8, 16, 128], P(('grp', 'sp'), 'tp'), parts along dimension 0
There are 2 independent parts, one for each index of `grp`. A program takes and returns all parts, laid end to end along the dimension named above; an argument that names none is the same for every part. Nothing has to cross between parts.
All inputs are finite; a program needn't handle non-finite values.
Results may differ from a plain program's by a relative error of at most 0.018.
The roundings to bfloat16 on the way count: a program that leaves them out, or rounds other values in their place, can miss the bound.
Values may be sent and summed in bfloat16 or wider, within the bound.
A program may use at most 64 MiB of HBM per device.

v0:
```python
import jax
import jax.numpy as jnp
from jax import lax
from jax.sharding import PartitionSpec as P

norm_epsilon = 1e-06
rope_base = 10000.0


def rotate(values, positions):
    half_width = values.shape[-1] // 2
    frequency = 1.0 / rope_base ** (
        jnp.arange(0, 2 * half_width, 2, dtype=jnp.float32) / (2 * half_width)
    )
    angles = positions[..., None] * frequency
    cosine = jnp.cos(angles)
    sine_part = jnp.sin(angles)
    front_half = values[..., :half_width]
    back_half = values[..., half_width:]
    return jnp.concatenate(
        [front_half * cosine - back_half * sine_part, front_half * sine_part + back_half * cosine],
        axis=-1,
    )


def local(tokens, kv_down, rope_down, kv_gain, key_up, value_up, query_nope, query_rope):
    seq_local, pos_dev, model_width = tokens.shape
    sp_count = lax.axis_size("sp")
    tp_count = lax.axis_size("tp")
    head_count = key_up.shape[1]
    heads_dev = head_count // tp_count
    seq_length = pos_dev * sp_count
    latent_width = kv_down.shape[1]
    rope_width = rope_down.shape[1]
    key_width = key_up.shape[2]
    sp_index = lax.axis_index("sp")
    tp_index = lax.axis_index("tp")
    head_start = tp_index * heads_dev
    flat_rows = tokens.reshape(seq_local * pos_dev, model_width)
    latent = jnp.dot(flat_rows, kv_down, preferred_element_type=jnp.float32)
    normed = (
        latent
        * lax.rsqrt(jnp.mean(latent * latent, axis=-1, keepdims=True) + norm_epsilon)
        * kv_gain
    ).astype(jnp.bfloat16)
    normed = normed.reshape(seq_local, pos_dev, latent_width)
    positions = (sp_index * pos_dev + jnp.arange(pos_dev, dtype=jnp.int32)).astype(jnp.float32)
    rope_raw = jnp.dot(flat_rows, rope_down, preferred_element_type=jnp.float32).reshape(
        seq_local, pos_dev, rope_width
    )
    rope_key = rotate(rope_raw, positions).astype(jnp.bfloat16)
    latent_all, rope_all = (
        lax.all_gather(normed, "tp", axis=0, tiled=True),
        lax.all_gather(rope_key, "tp", axis=0, tiled=True),
    )
    latent_mine, rope_mine = (
        lax.all_to_all(latent_all, "sp", split_axis=0, concat_axis=1, tiled=True),
        lax.all_to_all(rope_all, "sp", split_axis=0, concat_axis=1, tiled=True),
    )
    key_mine = lax.dynamic_slice_in_dim(key_up, head_start, heads_dev, 1)
    value_mine = lax.dynamic_slice_in_dim(value_up, head_start, heads_dev, 1)
    key_cache = jnp.einsum(
        "spc,chd->shpd", latent_mine, key_mine, preferred_element_type=jnp.float32
    ).astype(jnp.bfloat16)
    value_cache = jnp.einsum(
        "spc,chd->shpd", latent_mine, value_mine, preferred_element_type=jnp.float32
    ).astype(jnp.bfloat16)
    score_scale = (key_width + rope_width) ** (-0.5)
    query_pos = jnp.full((heads_dev,), float(seq_length), dtype=jnp.float32)
    rotated = rotate(query_rope.astype(jnp.float32), query_pos).astype(jnp.bfloat16)
    scores = jnp.einsum("shd,shld->shl", query_nope, key_cache, preferred_element_type=jnp.float32)
    scores = scores + jnp.einsum(
        "shr,slr->shl", rotated, rope_mine, preferred_element_type=jnp.float32
    )
    scores = scores * score_scale
    row_max = jnp.max(scores, axis=-1, keepdims=True)
    expo_terms = jnp.exp(scores - row_max)
    weights = expo_terms / jnp.sum(expo_terms, axis=-1, keepdims=True)
    read_out = jnp.einsum("shl,shld->shd", weights, value_cache.astype(jnp.float32)).astype(
        jnp.bfloat16
    )
    return (key_cache, value_cache, rope_mine, read_out)


def solution(mesh):
    placed = (
        P(("grp", "tp"), "sp", None),
        P(),
        P(),
        P(),
        P(),
        P(),
        P(("grp", "sp"), "tp", None),
        P(("grp", "sp"), "tp", None),
    )
    return jax.shard_map(
        local,
        mesh=mesh,
        in_specs=placed,
        out_specs=(
            P(("grp", "sp"), "tp", None, None),
            P(("grp", "sp"), "tp", None, None),
            P(("grp", "sp"), None, None),
            P(("grp", "sp"), "tp", None),
        ),
        check_vma=False,
    )
```

profile of v0, /device:TPU:0, one launch (start us, length us, event | category | flops | bytes accessed | tf_op | source)
XLA Modules:
  0.0 78.0 jit_solution(8015833157237881686)
XLA Ops:
  7.2 0.0 copy-start
  7.2 0.0 all-gather.3.cloned.1.call-start
  7.3 1.5 %copy-done = bf16[2048,512]{1,0:T(8,128)(2,1)S(1)} copy-done((bf16[2048,512]{1,0:T(8,128)(2,1)S(1)}, bf16[2048,512]{1,0:T(8,128)(2,1)}, u32[]{:S(2)}) %copy-start) | copy-done | bytes 2097176
  8.8 2.0 %multiply_reduce_fusion = (f32[256]{0:T(256)S(1)}, f32[256,512]{1,0:T(8,128)S(1)}) fusion(bf16[2048,512]{1,0:T(8,128)(2,1)S(1)} %copy-done, bf16[1,256,2048]{2,1,0:T(8,128)(2,1)} %param.8), kind=kOutput, calls=%fused_computation.15 | convolution fusion | flops 537132800 | bytes 3671040 | tf_op jit(solution)/shard_map/dot_general | solution.py:40
  10.8 0.8 %multiply_convert_fusion = bf16[256,512]{1,0:T(8,128)(2,1)} fusion(f32[256,512]{1,0:T(8,128)S(1)} %get-tuple-element.21, f32[512]{0:T(512)S(1)} %copy-done.8, f32[256]{0:T(256)S(1)} %add_rsqrt_fusion), kind=kLoop, calls=%fused_computation.14 | loop fusion | flops 393216 | bytes 789504 | tf_op jit(solution)/shard_map/convert_element_type | solution.py:45
  11.6 0.0 all-gather.3.cloned.1.call-update
  11.7 0.0 copy-start.9
  11.7 0.4 convolution_bitcast_fusion
  12.2 0.2 fusion.15
  12.4 15.3 %all_gather.7 = bf16[4,256,64]{1,2,0:T(8,128)(2,1)S(1)} all-gather(bf16[1,256,64]{1,2,0:T(8,128)(2,1)S(1)} %pad_maximum_fusion), channel_id=1, replica_groups=mesh['grp'=2,'sp'=4,'tp'=4] {'tp'}, dimensions={0}, use_global_device_ids=true | all-gather | bytes 163840 | tf_op jit(solution)/shard_map/all_gather | solution.py:54
  27.7 7.2 %all_to_all.21 = bf16[4,256,64]{1,2,0:T(8,128)(2,1)S(1)} all-to-all(bf16[4,256,64]{1,2,0:T(8,128)(2,1)S(1)} %all_gather.7), channel_id=1, replica_groups=mesh['grp'=2,'sp'=4,'tp'=4] {'sp'}, dimensions={0} | all-to-all | bytes 262144 | tf_op jit(solution)/shard_map/all_to_all | solution.py:58
  34.9 8.0 %all-gather.3.cloned.1.call-done = bf16[1024,512]{1,0:T(8,128)(2,1)} async-done(((bf16[256,512]{1,0:T(8,128)(2,1)}), bf16[1024,512]{1,0:T(8,128)(2,1)}) %all-gather.3.cloned.1.call-update) | async-done | bytes 1048592 | tf_op jit(solution)/shard_map/all_gather | solution.py:53
  42.9 3.5 %all-to-all-start = ((bf16[4,256,512]{2,1,0:T(8,128)(2,1)}), bf16[4,256,512]{2,1,0:T(8,128)(2,1)S(1)}, u32[]{:S(2)}, u32[]{:S(2)}) async-start(bf16[4,256,512]{2,1,0:T(8,128)(2,1)} %bitcast.53), calls=%async_computation | async-start | bytes 2097152 | tf_op jit(solution)/shard_map/all_to_all | solution.py:57
  46.5 3.1 %constant_dynamic-slice_fusion = (bf16[512,4,128]{2,1,0:T(4,128)(2,1)}, bf16[512,4,128]{2,1,0:T(4,128)(2,1)}) fusion(bf16[512,16,128]{2,1,0:T(8,128)(2,1)} %param.13, s32[]{:T(128)S(6)} %select_n.4, bf16[512,16,128]{2,1,0:T(8,128)(2,1)} %param.12), kind=kLoop, calls=%fused_computation.43 | loop fusion | bytes 2097156 | tf_op jit(solution)/shard_map/dynamic_slice | solution.py:61
  49.5 0.1 fusion.24
  49.6 0.1 copy.24
  49.7 0.7 all_to_all.8
  50.5 10.3 %all-to-all-done = bf16[4,256,512]{2,1,0:T(8,128)(2,1)S(1)} async-done(((bf16[4,256,512]{2,1,0:T(8,128)(2,1)}), bf16[4,256,512]{2,1,0:T(8,128)(2,1)S(1)}, u32[]{:S(2)}, u32[]{:S(2)}) %all-to-all-start) | async-done | bytes 1048608 | tf_op jit(solution)/shard_map/all_to_all | solution.py:57
  60.8 1.0 %copy-done.3 = bf16[4,256,512]{2,1,0:T(8,128)(2,1)} copy-done((bf16[4,256,512]{2,1,0:T(8,128)(2,1)}, bf16[4,256,512]{2,1,0:T(8,128)(2,1)S(1)}, u32[]{:S(2)}) %copy-start.3) | copy-done | bytes 1048600
  61.8 2.3 %convolution_convert_fusion.1 = bf16[4,128,1024]{2,1,0:T(8,128)(2,1)S(1)} fusion(bf16[1024,512,1]{1,0,2:T(8,128)(2,1)} %bitcast.54, bf16[512,4,128]{2,1,0:T(4,128)(2,1)} %get-tuple-element.25), kind=kOutput, calls=%fused_computation.1 | convolution fusion | flops 537395200 | bytes 2621440 | tf_op jit(solution)/shard_map/spc,chd->shpd/dot_general | solution.py:62
  64.0 0.0 copy-done.7
  64.0 0.2 fusion.3
  64.3 0.3 fusion.27
  64.6 0.2 fusion.19
  64.8 0.1 divide_bitcast_fusion
  64.9 0.8 convolution_convert_fusion
  65.7 0.0 copy-start.1
  65.7 1.0 %copy-done.1 = bf16[4,128,1024]{2,1,0:T(8,128)(2,1)} copy-done((bf16[4,128,1024]{2,1,0:T(8,128)(2,1)}, bf16[4,128,1024]{2,1,0:T(8,128)(2,1)S(1)}, u32[]{:S(2)}) %copy-start.1) | copy-done | bytes 1048600
  66.7 0.4 fusion.1
  67.0 0.6 convert_bitcast_fusion
  67.6 2.3 %copy.27 = bf16[1,4,1024,128]{3,2,1,0:T(8,128)(2,1)} copy(bf16[1,4,1024,128]{2,3,1,0:T(8,128)(2,1)} %bitcast.51) | data formatting | bytes 2097152
  69.9 1.3 %copy.26 = bf16[1,4,1024,128]{3,2,1,0:T(8,128)(2,1)} copy(bf16[1,4,1024,128]{2,3,1,0:T(8,128)(2,1)S(1)} %bitcast.50) | data formatting | bytes 2097152
  (20 shorter events, 0.1 us)
Async XLA Ops:
  7.2 1.6 %copy-start = (bf16[2048,512]{1,0:T(8,128)(2,1)S(1)}, bf16[2048,512]{1,0:T(8,128)(2,1)}, u32[]{:S(2)}) copy-start(bf16[2048,512]{1,0:T(8,128)(2,1)} %param.9) | copy-start | bytes 6291460
  7.2 4.5 %copy-start.2 = (bf16[1,256,2048]{2,1,0:T(8,128)(2,1)S(1)}, bf16[1,256,2048]{2,1,0:T(8,128)(2,1)}, u32[]{:S(2)}) copy-start(bf16[1,256,2048]{2,1,0:T(8,128)(2,1)} %param.8) | copy-start | bytes 3145732
  7.2 3.6 %copy-start.8 = (f32[512]{0:T(512)S(1)}, f32[512]{0:T(512)}, u32[]{:S(2)}) copy-start(f32[512]{0:T(512)} %param.11) | copy-start | bytes 6148
  7.2 4.5 %copy-start.6 = (bf16[2048,64]{0,1:T(8,128)(2,1)S(1)}, bf16[2048,64]{0,1:T(8,128)(2,1)}, u32[]{:S(2)}) copy-start(bf16[2048,64]{0,1:T(8,128)(2,1)} %param.10) | copy-start | bytes 786436
  7.2 35.7 %all-gather.3.cloned.1.call-start = ((), (), s32[]{:S(2)}) async-start(), calls=%async_computation.2 | async-start | bytes 1310720 | tf_op jit(solution)/shard_map/all_gather | solution.py:53
  11.7 34.7 %copy-start.9 = (bf16[1,4,64]{2,1,0:T(4,128)(2,1)S(1)}, bf16[1,4,64]{2,1,0:T(4,128)(2,1)}, u32[]{:S(2)}) copy-start(bf16[1,4,64]{2,1,0:T(4,128)(2,1)} %param.15) | copy-start | bytes 1540
  42.9 17.9 %all-to-all-start = ((bf16[4,256,512]{2,1,0:T(8,128)(2,1)}), bf16[4,256,512]{2,1,0:T(8,128)(2,1)S(1)}, u32[]{:S(2)}, u32[]{:S(2)}) async-start(bf16[4,256,512]{2,1,0:T(8,128)(2,1)} %bitcast.53), calls=%async_computation | async-start | bytes 2097152 | tf_op jit(solution)/shard_map/all_to_all | solution.py:57
  49.5 14.5 %copy-start.7 = (bf16[1,4,128]{2,1,0:T(4,128)(2,1)S(1)}, bf16[1,4,128]{2,1,0:T(4,128)(2,1)}, u32[]{:S(2)}) copy-start(bf16[1,4,128]{2,1,0:T(4,128)(2,1)} %param.14) | copy-start | bytes 3076
  60.8 1.0 %copy-start.3 = (bf16[4,256,512]{2,1,0:T(8,128)(2,1)}, bf16[4,256,512]{2,1,0:T(8,128)(2,1)S(1)}, u32[]{:S(2)}) copy-start(bf16[4,256,512]{2,1,0:T(8,128)(2,1)S(1)} %all-to-all-done) | copy-start | bytes 3145732
  61.8 3.1 %copy-start.4 = (bf16[4,256,512]{2,1,0:T(8,128)(2,1)S(1)}, bf16[4,256,512]{2,1,0:T(8,128)(2,1)}, u32[]{:S(2)}) copy-start(bf16[4,256,512]{2,1,0:T(8,128)(2,1)} %copy-done.3) | copy-start | bytes 3145732
  61.8 3.2 %copy-start.5 = (bf16[512,4,128]{2,1,0:T(4,128)(2,1)S(1)}, bf16[512,4,128]{2,1,0:T(4,128)(2,1)}, u32[]{:S(2)}) copy-start(bf16[512,4,128]{2,1,0:T(4,128)(2,1)} %get-tuple-element.24) | copy-start | bytes 1572868
  65.7 1.0 %copy-start.1 = (bf16[4,128,1024]{2,1,0:T(8,128)(2,1)}, bf16[4,128,1024]{2,1,0:T(8,128)(2,1)S(1)}, u32[]{:S(2)}) copy-start(bf16[4,128,1024]{2,1,0:T(8,128)(2,1)S(1)} %convolution_convert_fusion) | copy-start | bytes 3145732
Sparse Core Ops, SparseCore 0:
  11.8 31.0 all-gather.2
where the time goes:
time: 78.3 us; the launch traced here: 78 us
  blocking collectives  22.5 us (29%)
  waiting for transfers between devices  18.3 us (23%)
  between operations  14.2 us (18%)
  local copies, waits for them, and re-layouts  11 us (14%)
  matrix products  6.41 us (8%)
  starting transfers between devices  3.55 us (5%)
  other arithmetic  2.06 us (3%)
    all_gather x1, blocking collectives, local(): lax.all_gather(rope_key, 'tp', axis=0, tiled=True)  15.3 us
    all_to_all x1, waiting for transfers between devices, local(): lax.all_to_all(latent_all, 'sp', split_axis=0, concat_axis=1, tiled=True)  10.3 us
    all_gather x1, waiting for transfers between devices, local(): lax.all_gather(normed, 'tp', axis=0, tiled=True)  7.97 us
    all_to_all x1, blocking collectives, local(): lax.all_to_all(rope_all, 'sp', split_axis=0, concat_axis=1, tiled=True)  7.19 us
    unnamed x22, local copies, waits for them, and re-layouts  7.05 us
    all_to_all x1, starting transfers between devices, local(): lax.all_to_all(latent_all, 'sp', split_axis=0, concat_axis=1, tiled=True)  3.51 us
    dynamic_slice x1, local copies, waits for them, and re-layouts, local(): value_mine = lax.dynamic_slice_in_dim(value_up, head_start, heads_dev, 1)  3.08 us
    dot_general x1, matrix products, local(): jnp.einsum('spc,chd->shpd', latent_mine, key_mine, preferred_element_type...  2.26 us
  transfers between devices with their start and end apart: 2, of which 2 were waited for; matrix products, arithmetic and copies ran while one was open for 5% of the time, Pallas kernels for 0%

commit v1 on v0

v1 whole, which is shorter than its diff:
```python
import functools

import jax
import jax.numpy as jnp
import numpy as np
from jax import lax
from jax.experimental import pallas as pl
from jax.experimental.pallas import tpu as pltpu
from jax.sharding import PartitionSpec as P

norm_epsilon = 1e-06
rope_base = 10000.0
MESH = pl.DeviceIdType.MESH
F32, BF16 = jnp.float32, jnp.bfloat16


def tables(length, width):
    frequency = (1.0 / rope_base ** (np.arange(0, width, 2, dtype=np.float64) / width)).astype(np.float32)
    angles = frequency[:, None] * np.arange(length, dtype=np.float32)[None, :]
    cached = np.stack([np.cos(angles.astype(np.float64)), np.sin(angles.astype(np.float64))])
    ask = (np.float32(length) * frequency).astype(np.float64)
    asked = np.stack([np.tile(np.cos(ask), 2), np.tile(np.sin(ask), 2)])
    return cached.astype(np.float32), asked.astype(np.float32)


def kernel(
    sp_count, tp_count, bounds, scale,
    tok, kvd, rpt, gain, kup, vup, qn, qr, tab, qtab,
    key_out, val_out, rope_out, read_out,
    box, tok_v, kvd_v, rpt_v, gain_v, up_v, wide, kw, vw, qn_v, qr_v, tab_v, qtab_v, scores,
    in_sem, zsend, zrecv, csend, crecv,
):
    me = lax.axis_index("sp")
    here = lax.axis_index("tp")
    seq_local, pos_dev, _ = tok.shape
    rope_width = rpt.shape[0]
    half = rope_width // 2
    heads_dev, key_width = qn.shape[1], qn.shape[2]
    rope_rows = bounds[0]
    pieces = [pl.ds(a, b - a) for a, b in zip((0,) + bounds[1:-1], bounds[1:])]
    count = len(pieces)
    last = tp_count - 1

    barrier = pltpu.get_barrier_semaphore()
    for step in range(1, sp_count):
        pl.semaphore_signal(
            barrier, inc=1, device_id={"sp": lax.rem(me + step, sp_count)}, device_id_type=MESH
        )
    if tp_count > 1:
        for step in (1, last):
            pl.semaphore_signal(
                barrier, inc=1, device_id={"tp": lax.rem(here + step, tp_count)}, device_id_type=MESH
            )

    tile = up_v.shape[2]
    head_start = here * heads_dev
    head_tile = pl.multiple_of(head_start // tile * tile, tile)
    head_off = lax.rem(head_start, tile)
    loads = [
        pltpu.make_async_copy(src, dst, in_sem.at[n])
        for n, (src, dst) in enumerate([
            (tok, tok_v),
            (kvd, kvd_v),
            (gain, gain_v),
            (rpt, rpt_v),
            (tab.at[:, :, pl.ds(pl.multiple_of(me * pos_dev, pos_dev), pos_dev)], tab_v),
            (kup.at[:, pl.ds(head_tile, tile), :], up_v.at[0]),
            (vup.at[:, pl.ds(head_tile, tile), :], up_v.at[1]),
            (qn, qn_v),
            (qr, qr_v),
            (qtab, qtab_v),
        ])
    ]
    for load in loads:
        load.start()

    def slot(prompt):
        return jnp.where(prompt == me, me, sp_count + prompt)

    for n in (3, 4, 0):
        loads[n].wait()
    for q in range(seq_local):
        mine = slot(here * seq_local + q)
        rows = tok_v[q]
        raw = lax.dot_general(rpt_v[...], rows, (((1,), (1,)), ((), ())), preferred_element_type=F32)
        cosine, sine_part = tab_v[0], tab_v[1]
        front, back = raw[:half], raw[half:]
        turned = jnp.concatenate(
            [front * cosine - back * sine_part, front * sine_part + back * cosine], axis=0
        ).astype(BF16)
        groups = rope_width // rope_rows
        box[mine, 0:rope_rows, :] = jnp.concatenate(
            [turned[g * rope_rows:(g + 1) * rope_rows] for g in range(groups)], axis=1
        )
    for n in (1, 2):
        loads[n].wait()
    for q in range(seq_local):
        mine = slot(here * seq_local + q)
        latent = jnp.dot(tok_v[q], kvd_v[...], preferred_element_type=F32)
        normed = (
            latent
            * lax.rsqrt(jnp.mean(latent * latent, axis=-1, keepdims=True) + norm_epsilon)
            * gain_v[...]
        ).astype(BF16)
        box[mine, rope_rows:rope_rows + pos_dev, :] = normed

    def along(prompt, way, hop, q, s):
        part = box.at[slot(prompt), pieces[s]]
        return pltpu.make_async_remote_copy(
            src_ref=part, dst_ref=part,
            send_sem=zsend.at[way, hop, q, s], recv_sem=zrecv.at[way, hop, q, s],
            device_id={"tp": here + (1 if way == 0 else -1)}, device_id_type=MESH,
        )

    def across(prompt, s):
        return pltpu.make_async_remote_copy(
            src_ref=box.at[slot(prompt), pieces[s]], dst_ref=box.at[me, pieces[s]],
            send_sem=csend.at[prompt, s], recv_sem=crecv.at[me, s],
            device_id={"sp": prompt}, device_id_type=MESH,
        )

    pl.semaphore_wait(barrier, sp_count - 1 + (2 if tp_count > 1 else 0))
    inner = {0: here < last, 1: here > 0}
    for q in range(seq_local):
        prompt = here * seq_local + q
        for s in range(count):
            for way in (0, 1):
                @pl.when(inner[way])
                def _(way=way, s=s):
                    along(prompt, way, 0, q, s).start()

            @pl.when(prompt != me)
            def _(s=s):
                across(prompt, s).start()

    for n in (5, 6, 7, 8, 9):
        loads[n].wait()
    depth = up_v.shape[1]
    for n, target in enumerate((kw, vw)):
        wide[...] = up_v[n].astype(F32).reshape(depth * tile, key_width)
        for h in range(heads_dev):
            target[:, h * key_width:(h + 1) * key_width] = wide[
                pl.ds(head_off + h, depth, stride=tile), :
            ].astype(BF16)

    for hop in range(last):
        for q in range(seq_local):
            for s in range(count):
                for way in (0, 1):
                    owner = here - 1 - hop if way == 0 else here + 1 + hop
                    has = owner >= 0 if way == 0 else owner <= last

                    @pl.when(has)
                    def _(way=way, s=s, owner=owner):
                        prompt = owner * seq_local + q
                        along(prompt, way, hop, q, s).wait_recv()
                        if hop + 1 < last:
                            @pl.when(inner[way])
                            def _():
                                along(prompt, way, hop + 1, q, s).start()

                        @pl.when(prompt != me)
                        def _():
                            across(prompt, s).start()

    query = qn_v[0]
    zero = jnp.zeros_like(query)
    picks = lax.broadcasted_iota(jnp.int32, query.shape, 0)
    spread = jnp.concatenate(
        [jnp.where(picks == h, query.astype(F32), zero.astype(F32)) for h in range(heads_dev)], axis=1
    ).astype(BF16)
    ask = qr_v[0].astype(F32)
    swapped = jnp.concatenate([-ask[:, half:], ask[:, :half]], axis=1)
    rotated = (ask * qtab_v[0:1, :] + swapped * qtab_v[1:2, :]).astype(BF16)
    group_rows = pos_dev // 2
    for group in range(2):
        for step in range(sp_count):
            source = lax.rem(me + step, sp_count)
            if step:
                for s in ((0,) if group == 0 else range(1, count)):
                    part = box.at[source, pieces[s]]
                    pltpu.make_async_remote_copy(
                        src_ref=part, dst_ref=part,
                        send_sem=csend.at[source, s], recv_sem=crecv.at[source, s],
                        device_id={"sp": source}, device_id_type=MESH,
                    ).wait_recv()
            block = pl.ds(pl.multiple_of(source * pos_dev, pos_dev), pos_dev)
            if group == 0:
                packed = box[source, 0:rope_rows, :]
                turned = jnp.concatenate(
                    [packed[:, g * pos_dev:(g + 1) * pos_dev] for g in range(rope_width // rope_rows)], axis=0
                )
                rope_out[0, :, block] = turned
            begin = rope_rows + group * group_rows
            rows = box[source, begin:begin + group_rows, :]
            place = pl.ds(pl.multiple_of(source * pos_dev + group * group_rows, group_rows), group_rows)
            keys = jnp.dot(rows, kw[...], preferred_element_type=F32).astype(BF16)
            values = jnp.dot(rows, vw[...], preferred_element_type=F32).astype(BF16)
            for h in range(heads_dev):
                key_out[0, h, place, :] = keys[:, h * key_width:(h + 1) * key_width]
                val_out[0, h, place, :] = values[:, h * key_width:(h + 1) * key_width]
            scores[:, place] = lax.dot_general(
                spread, keys, (((1,), (1,)), ((), ())), preferred_element_type=F32
            )

    total = scores[...] + jnp.dot(rotated, rope_out[0], preferred_element_type=F32)
    total = total * scale
    terms = jnp.exp(total - jnp.max(total, axis=-1, keepdims=True))
    weights = terms / jnp.sum(terms, axis=-1, keepdims=True)
    high = weights.astype(BF16)
    low = (weights - high.astype(F32)).astype(BF16)
    both = jnp.concatenate([high.astype(F32), low.astype(F32)], axis=0).astype(BF16)
    reads = []
    for h in range(heads_dev):
        read = jnp.dot(both, val_out[0, h], preferred_element_type=F32)
        reads.append(read[h:h + 1] + read[heads_dev + h:heads_dev + h + 1])
    read_out[0] = jnp.concatenate(reads, axis=0).astype(BF16)

    for hop in range(last):
        for q in range(seq_local):
            for s in range(count):
                for way in (0, 1):
                    owner = here - hop if way == 0 else here + hop
                    has = owner >= 0 if way == 0 else owner <= last

                    @pl.when(jnp.logical_and(has, inner[way]))
                    def _(way=way, s=s, owner=owner):
                        along(owner * seq_local + q, way, hop, q, s).wait_send()
    for step in range(1, sp_count):
        prompt = lax.rem(me + step, sp_count)
        for s in range(count):
            across(prompt, s).wait_send()


def local(tokens, kv_down, rope_down, kv_gain, key_up, value_up, query_nope, query_rope):
    seq_local, pos_dev, model_width = tokens.shape
    sp_count = lax.axis_size("sp")
    tp_count = lax.axis_size("tp")
    latent_width = kv_down.shape[1]
    rope_width = rope_down.shape[1]
    head_count, key_width = key_up.shape[1], key_up.shape[2]
    heads_dev = head_count // tp_count
    length = pos_dev * sp_count
    rope_rows = rope_width * pos_dev // latent_width
    rows = rope_rows + pos_dev
    bounds = (rope_rows, rope_rows + pos_dev // 2, rope_rows + pos_dev * 3 // 4, rows)
    prompts = tp_count * seq_local
    cached, asked = tables(length, rope_width)
    tile = 8
    any_space = pl.BlockSpec(memory_space=pl.ANY)
    vmem = pl.BlockSpec(memory_space=pltpu.VMEM)
    hops = max(tp_count - 1, 1)
    count = len(bounds) - 1
    dma = pltpu.SemaphoreType.DMA
    key_cache, value_cache, rope_t, read_out = pl.pallas_call(
        functools.partial(kernel, sp_count, tp_count, bounds, (key_width + rope_width) ** (-0.5)),
        out_shape=(
            jax.ShapeDtypeStruct((1, heads_dev, length, key_width), BF16),
            jax.ShapeDtypeStruct((1, heads_dev, length, key_width), BF16),
            jax.ShapeDtypeStruct((1, rope_width, length), BF16),
            jax.ShapeDtypeStruct((1, heads_dev, key_width), BF16),
        ),
        in_specs=[any_space] * 10,
        out_specs=(vmem,) * 4,
        scratch_shapes=[
            pltpu.VMEM((sp_count + prompts, rows, latent_width), BF16),
            pltpu.VMEM(tokens.shape, BF16),
            pltpu.VMEM(kv_down.shape, BF16),
            pltpu.VMEM((rope_width, model_width), BF16),
            pltpu.VMEM((1, latent_width), F32),
            pltpu.VMEM((2, latent_width, tile, key_width), BF16),
            pltpu.VMEM((latent_width * tile, key_width), F32),
            pltpu.VMEM((latent_width, heads_dev * key_width), BF16),
            pltpu.VMEM((latent_width, heads_dev * key_width), BF16),
            pltpu.VMEM(query_nope.shape, BF16),
            pltpu.VMEM(query_rope.shape, BF16),
            pltpu.VMEM((2, rope_width // 2, pos_dev), F32),
            pltpu.VMEM((2, rope_width), F32),
            pltpu.VMEM((heads_dev, length), F32),
            dma((10,)),
            dma((2, hops, seq_local, count)),
            dma((2, hops, seq_local, count)),
            dma((prompts, count)),
            dma((sp_count, count)),
        ],
        compiler_params=pltpu.CompilerParams(
            collective_id=0, has_side_effects=True, vmem_limit_bytes=40 * 1024 * 1024
        ),
    )(
        tokens, kv_down, rope_down.T, kv_gain.reshape(1, latent_width), key_up, value_up,
        query_nope, query_rope, jnp.asarray(cached), jnp.asarray(asked),
    )
    return (key_cache, value_cache, jnp.swapaxes(rope_t, 1, 2), read_out)


def solution(mesh):
    placed = (
        P(("grp", "tp"), "sp", None),
        P(),
        P(),
        P(),
        P(),
        P(),
        P(("grp", "sp"), "tp", None),
        P(("grp", "sp"), "tp", None),
    )
    return jax.shard_map(
        local,
        mesh=mesh,
        in_specs=placed,
        out_specs=(
            P(("grp", "sp"), "tp", None, None),
            P(("grp", "sp"), "tp", None, None),
            P(("grp", "sp"), None, None),
            P(("grp", "sp"), "tp", None),
        ),
        check_vma=False,
    )
```

time: 78.3 us -> 44.6 us (0.57)
  the two profiles are of different devices: /device:TPU:0 before, /device:TPU:5 now
where the time goes in v1:
time: 44.6 us; the launch traced here: 44.2 us
  Pallas kernels  29.8 us (67%)
  local copies, waits for them, and re-layouts  13.8 us (31%)
  between operations  0.66 us (1%)
    pallas_call x1, Pallas kernels, local(): pl.pallas_call(functools.partial(kernel, sp_count, tp_count, bounds, (key...  29.8 us
    unnamed x24, local copies, waits for them, and re-layouts  13.8 us

profile of v1, /device:TPU:5, one launch (start us, length us, event | category | flops | bytes accessed | tf_op | source)
XLA Modules:
  0.0 44.2 jit_solution(12074850518504718604)
XLA Ops:
  0.6 0.0 copy-start
  0.6 1.6 %copy-done = bf16[2048,512]{1,0:T(8,128)(2,1)S(1)} copy-done((bf16[2048,512]{1,0:T(8,128)(2,1)S(1)}, bf16[2048,512]{1,0:T(8,128)(2,1)}, u32[]{:S(2)}) %copy-start) | copy-done | bytes 2097176
  2.2 0.0 copy-start.1
  2.2 1.6 %copy-done.1 = bf16[512,16,128]{2,1,0:T(8,128)(2,1)S(1)} copy-done((bf16[512,16,128]{2,1,0:T(8,128)(2,1)S(1)}, bf16[512,16,128]{2,1,0:T(8,128)(2,1)}, u32[]{:S(2)}) %copy-start.1) | copy-done | bytes 2097176
  3.8 0.0 copy-start.2
  3.8 1.6 %copy-done.2 = bf16[512,16,128]{2,1,0:T(8,128)(2,1)S(1)} copy-done((bf16[512,16,128]{2,1,0:T(8,128)(2,1)S(1)}, bf16[512,16,128]{2,1,0:T(8,128)(2,1)}, u32[]{:S(2)}) %copy-start.2) | copy-done | bytes 2097176
  5.4 0.0 copy-start.3
  5.4 1.2 %copy-done.3 = bf16[1,256,2048]{2,1,0:T(8,128)(2,1)S(1)} copy-done((bf16[1,256,2048]{2,1,0:T(8,128)(2,1)S(1)}, bf16[1,256,2048]{2,1,0:T(8,128)(2,1)}, u32[]{:S(2)}) %copy-start.3) | copy-done | bytes 1048600
  6.6 0.0 copy-start.4
  6.6 0.9 %copy-done.4 = bf16[2048,64]{0,1:T(8,128)(2,1)S(1)} copy-done((bf16[2048,64]{0,1:T(8,128)(2,1)S(1)}, bf16[2048,64]{0,1:T(8,128)(2,1)}, u32[]{:S(2)}) %copy-start.4) | copy-done | bytes 262168
  7.6 0.0 copy-start.5
  7.6 0.9 %copy-done.5 = f32[2,32,1024]{2,1,0:T(8,128)S(1)} copy-done((f32[2,32,1024]{2,1,0:T(8,128)S(1)}, f32[2,32,1024]{2,1,0:T(8,128)}, u32[]{:S(2)}) %copy-start.5) | copy-done | bytes 262168
  8.5 0.0 copy-start.6
  8.5 0.7 %copy-done.6 = f32[512]{0:T(512)S(1)} copy-done((f32[512]{0:T(512)S(1)}, f32[512]{0:T(512)}, u32[]{:S(2)}) %copy-start.6) | copy-done | bytes 2072
  9.2 0.0 copy-start.7
  9.2 0.7 %copy-done.7 = bf16[1,4,128]{2,1,0:T(4,128)(2,1)S(1)} copy-done((bf16[1,4,128]{2,1,0:T(4,128)(2,1)S(1)}, bf16[1,4,128]{2,1,0:T(4,128)(2,1)}, u32[]{:S(2)}) %copy-start.7) | copy-done | bytes 1048
  9.9 0.0 copy-start.8
  9.9 0.7 %copy-done.8 = bf16[1,4,64]{2,1,0:T(4,128)(2,1)S(1)} copy-done((bf16[1,4,64]{2,1,0:T(4,128)(2,1)S(1)}, bf16[1,4,64]{2,1,0:T(4,128)(2,1)}, u32[]{:S(2)}) %copy-start.8) | copy-done | bytes 536
  10.6 0.0 copy-start.9
  10.6 0.7 %copy-done.9 = f32[2,64]{1,0:T(2,128)S(1)} copy-done((f32[2,64]{1,0:T(2,128)S(1)}, f32[2,64]{1,0:T(2,128)}, u32[]{:S(2)}) %copy-start.9) | copy-done | bytes 536
  11.3 29.8 %shard_map.129 = (bf16[1,4,1024,128]{3,2,1,0:T(8,128)(2,1)S(1)}, bf16[1,4,1024,128]{3,2,1,0:T(8,128)(2,1)S(1)}, bf16[1,64,1024]{2,1,0:T(8,128)(2,1)S(1)}, bf16[1,4,128]{2,1,0:T(4,128)(2,1)S(1)}) custom-call(bf16[1,256,2048]{2,1,0:T(8,128)(2,1)S(1)} %copy-done.3, bf16[2048,512]{1,0:T(8,128)(2,1)S(1)} %copy-done, bf16[64,2048]{1,0:T(8,128)(2,1)S(1)} %bitcast.3, ...), custom_call_target="tpu_custom_call" | custom-call | tf_op jit(solution)/shard_map/pallas_call | solution.py:255
  41.1 1.0 %copy.18 = bf16[1,4,1024,128]{3,2,1,0:T(8,128)(2,1)} copy(bf16[1,4,1024,128]{3,2,1,0:T(8,128)(2,1)S(1)} %get-tuple-element.16) | data formatting | bytes 2097152
  42.0 1.0 %copy.19 = bf16[1,4,1024,128]{3,2,1,0:T(8,128)(2,1)} copy(bf16[1,4,1024,128]{3,2,1,0:T(8,128)(2,1)S(1)} %get-tuple-element.17) | data formatting | bytes 2097152
  43.0 0.7 %copy.20 = bf16[1,1024,64]{1,2,0:T(8,128)(2,1)} copy(bf16[1,1024,64]{1,2,0:T(8,128)(2,1)S(1)} %bitcast.4) | data formatting | bytes 262144
  43.7 0.6 %copy.21 = bf16[1,4,128]{2,1,0:T(4,128)(2,1)} copy(bf16[1,4,128]{2,1,0:T(4,128)(2,1)S(1)} %get-tuple-element.19) | data formatting | bytes 2048
Async XLA Ops:
  0.6 1.6 %copy-start = (bf16[2048,512]{1,0:T(8,128)(2,1)S(1)}, bf16[2048,512]{1,0:T(8,128)(2,1)}, u32[]{:S(2)}) copy-start(bf16[2048,512]{1,0:T(8,128)(2,1)} %kvd.1) | copy-start | bytes 6291460
  2.2 1.6 %copy-start.1 = (bf16[512,16,128]{2,1,0:T(8,128)(2,1)S(1)}, bf16[512,16,128]{2,1,0:T(8,128)(2,1)}, u32[]{:S(2)}) copy-start(bf16[512,16,128]{2,1,0:T(8,128)(2,1)} %kup.1) | copy-start | bytes 6291460
  3.8 1.6 %copy-start.2 = (bf16[512,16,128]{2,1,0:T(8,128)(2,1)S(1)}, bf16[512,16,128]{2,1,0:T(8,128)(2,1)}, u32[]{:S(2)}) copy-start(bf16[512,16,128]{2,1,0:T(8,128)(2,1)} %vup.1) | copy-start | bytes 6291460
  5.4 1.2 %copy-start.3 = (bf16[1,256,2048]{2,1,0:T(8,128)(2,1)S(1)}, bf16[1,256,2048]{2,1,0:T(8,128)(2,1)}, u32[]{:S(2)}) copy-start(bf16[1,256,2048]{2,1,0:T(8,128)(2,1)} %tok.1) | copy-start | bytes 3145732
  6.6 0.9 %copy-start.4 = (bf16[2048,64]{0,1:T(8,128)(2,1)S(1)}, bf16[2048,64]{0,1:T(8,128)(2,1)}, u32[]{:S(2)}) copy-start(bf16[2048,64]{0,1:T(8,128)(2,1)} %param.12) | copy-start | bytes 786436
  7.6 0.9 %copy-start.5 = (f32[2,32,1024]{2,1,0:T(8,128)S(1)}, f32[2,32,1024]{2,1,0:T(8,128)}, u32[]{:S(2)}) copy-start(f32[2,32,1024]{2,1,0:T(8,128)} %constant.4.clone.tab) | copy-start | bytes 786436
  8.5 0.7 %copy-start.6 = (f32[512]{0:T(512)S(1)}, f32[512]{0:T(512)}, u32[]{:S(2)}) copy-start(f32[512]{0:T(512)} %param.13) | copy-start | bytes 6148
  9.2 0.7 %copy-start.7 = (bf16[1,4,128]{2,1,0:T(4,128)(2,1)S(1)}, bf16[1,4,128]{2,1,0:T(4,128)(2,1)}, u32[]{:S(2)}) copy-start(bf16[1,4,128]{2,1,0:T(4,128)(2,1)} %qn.1) | copy-start | bytes 3076
  9.9 0.7 %copy-start.8 = (bf16[1,4,64]{2,1,0:T(4,128)(2,1)S(1)}, bf16[1,4,64]{2,1,0:T(4,128)(2,1)}, u32[]{:S(2)}) copy-start(bf16[1,4,64]{2,1,0:T(4,128)(2,1)} %qr.1) | copy-start | bytes 1540
  10.6 0.7 %copy-start.9 = (f32[2,64]{1,0:T(2,128)S(1)}, f32[2,64]{1,0:T(2,128)}, u32[]{:S(2)}) copy-start(f32[2,64]{1,0:T(2,128)} %constant.5.clone.qtab) | copy-start | bytes 1540

commit v2 on v1

--- a/solution.py
+++ b/solution.py
@@ -24,10 +24,10 @@
 
 
 def kernel(
-    sp_count, tp_count, bounds, scale,
-    tok, kvd, rpt, gain, kup, vup, qn, qr, tab, qtab,
-    key_out, val_out, rope_out, read_out,
-    box, tok_v, kvd_v, rpt_v, gain_v, up_v, wide, kw, vw, qn_v, qr_v, tab_v, qtab_v, scores,
+    sp_count, tp_count, heads_dev, bounds,
+    tok, kvd, rpt, gain, kup, vup, tab,
+    key_out, val_out, rope_out,
+    box, tok_v, kvd_v, rpt_v, gain_v, up_v, wide, kw, vw, tab_v,
     in_sem, zsend, zrecv, csend, crecv,
 ):
     me = lax.axis_index("sp")
@@ -35,7 +35,7 @@
     seq_local, pos_dev, _ = tok.shape
     rope_width = rpt.shape[0]
     half = rope_width // 2
-    heads_dev, key_width = qn.shape[1], qn.shape[2]
+    key_width = kup.shape[2]
     rope_rows = bounds[0]
     pieces = [pl.ds(a, b - a) for a, b in zip((0,) + bounds[1:-1], bounds[1:])]
     count = len(pieces)
@@ -66,9 +66,6 @@
             (tab.at[:, :, pl.ds(pl.multiple_of(me * pos_dev, pos_dev), pos_dev)], tab_v),
             (kup.at[:, pl.ds(head_tile, tile), :], up_v.at[0]),
             (vup.at[:, pl.ds(head_tile, tile), :], up_v.at[1]),
-            (qn, qn_v),
-            (qr, qr_v),
-            (qtab, qtab_v),
         ])
     ]
     for load in loads:
@@ -92,18 +89,6 @@
         box[mine, 0:rope_rows, :] = jnp.concatenate(
             [turned[g * rope_rows:(g + 1) * rope_rows] for g in range(groups)], axis=1
         )
-    for n in (1, 2):
-        loads[n].wait()
-    for q in range(seq_local):
-        mine = slot(here * seq_local + q)
-        latent = jnp.dot(tok_v[q], kvd_v[...], preferred_element_type=F32)
-        normed = (
-            latent
-            * lax.rsqrt(jnp.mean(latent * latent, axis=-1, keepdims=True) + norm_epsilon)
-            * gain_v[...]
-        ).astype(BF16)
-        box[mine, rope_rows:rope_rows + pos_dev, :] = normed
-
     def along(prompt, way, hop, q, s):
         part = box.at[slot(prompt), pieces[s]]
         return pltpu.make_async_remote_copy(
@@ -119,21 +104,39 @@
             device_id={"sp": prompt}, device_id_type=MESH,
         )
 
-    pl.semaphore_wait(barrier, sp_count - 1 + (2 if tp_count > 1 else 0))
     inner = {0: here < last, 1: here > 0}
-    for q in range(seq_local):
-        prompt = here * seq_local + q
-        for s in range(count):
-            for way in (0, 1):
-                @pl.when(inner[way])
-                def _(way=way, s=s):
-                    along(prompt, way, 0, q, s).start()
-
-            @pl.when(prompt != me)
-            def _(s=s):
-                across(prompt, s).start()
-
-    for n in (5, 6, 7, 8, 9):
+    for n in (1, 2):
+        loads[n].wait()
+    half_rows = pos_dev // 2
+    for group in range(2):
+        for q in range(seq_local):
+            mine = slot(here * seq_local + q)
+            latent = jnp.dot(
+                tok_v[q, group * half_rows:(group + 1) * half_rows, :], kvd_v[...],
+                preferred_element_type=F32,
+            )
+            normed = (
+                latent
+                * lax.rsqrt(jnp.mean(latent * latent, axis=-1, keepdims=True) + norm_epsilon)
+                * gain_v[...]
+            ).astype(BF16)
+            begin = rope_rows + group * half_rows
+            box[mine, begin:begin + half_rows, :] = normed
+        if group == 0:
+            pl.semaphore_wait(barrier, sp_count - 1 + (2 if tp_count > 1 else 0))
+        for q in range(seq_local):
+            prompt = here * seq_local + q
+            for s in ((0,) if group == 0 else range(1, count)):
+                for way in (0, 1):
+                    @pl.when(inner[way])
+                    def _(way=way, s=s):
+                        along(prompt, way, 0, q, s).start()
+
+                @pl.when(prompt != me)
+                def _(s=s):
+                    across(prompt, s).start()
+
+    for n in (5, 6):
         loads[n].wait()
     depth = up_v.shape[1]
     for n, target in enumerate((kw, vw)):
@@ -163,15 +166,6 @@
                         def _():
                             across(prompt, s).start()
 
-    query = qn_v[0]
-    zero = jnp.zeros_like(query)
-    picks = lax.broadcasted_iota(jnp.int32, query.shape, 0)
-    spread = jnp.concatenate(
-        [jnp.where(picks == h, query.astype(F32), zero.astype(F32)) for h in range(heads_dev)], axis=1
-    ).astype(BF16)
-    ask = qr_v[0].astype(F32)
-    swapped = jnp.concatenate([-ask[:, half:], ask[:, :half]], axis=1)
-    rotated = (ask * qtab_v[0:1, :] + swapped * qtab_v[1:2, :]).astype(BF16)
     group_rows = pos_dev // 2
     for group in range(2):
         for step in range(sp_count):
@@ -199,22 +193,6 @@
             for h in range(heads_dev):
                 key_out[0, h, place, :] = keys[:, h * key_width:(h + 1) * key_width]
                 val_out[0, h, place, :] = values[:, h * key_width:(h + 1) * key_width]
-            scores[:, place] = lax.dot_general(
-                spread, keys, (((1,), (1,)), ((), ())), preferred_element_type=F32
-            )
-
-    total = scores[...] + jnp.dot(rotated, rope_out[0], preferred_element_type=F32)
-    total = total * scale
-    terms = jnp.exp(total - jnp.max(total, axis=-1, keepdims=True))
-    weights = terms / jnp.sum(terms, axis=-1, keepdims=True)
-    high = weights.astype(BF16)
-    low = (weights - high.astype(F32)).astype(BF16)
-    both = jnp.concatenate([high.astype(F32), low.astype(F32)], axis=0).astype(BF16)
-    reads = []
-    for h in range(heads_dev):
-        read = jnp.dot(both, val_out[0, h], preferred_element_type=F32)
-        reads.append(read[h:h + 1] + read[heads_dev + h:heads_dev + h + 1])
-    read_out[0] = jnp.concatenate(reads, axis=0).astype(BF16)
 
     for hop in range(last):
         for q in range(seq_local):
@@ -230,6 +208,40 @@
         prompt = lax.rem(me + step, sp_count)
         for s in range(count):
             across(prompt, s).wait_send()
+
+
+def finish(scale, keys, vals, ropes, query, ask, qtab, key_out, val_out, rope_out, read_out, sem):
+    moves = [
+        pltpu.make_async_copy(src, dst, sem.at[n])
+        for n, (src, dst) in enumerate([(vals, val_out), (keys, key_out), (ropes, rope_out)])
+    ]
+    for move in moves:
+        move.start()
+    heads_dev = query.shape[1]
+    half = ask.shape[2] // 2
+    turn = ask[0].astype(F32)
+    swapped = jnp.concatenate([-turn[:, half:], turn[:, :half]], axis=1)
+    rotated = (turn * qtab[0:1, :] + swapped * qtab[1:2, :]).astype(BF16)
+    asked = query[0]
+    picks = []
+    for h in range(heads_dev):
+        full = lax.dot_general(
+            asked, keys[0, h], (((1,), (1,)), ((), ())), preferred_element_type=F32
+        )
+        picks.append(full[h:h + 1])
+    total = jnp.concatenate(picks, axis=0)
+    total = (total + jnp.dot(rotated, ropes[0], preferred_element_type=F32)) * scale
+    terms = jnp.exp(total - jnp.max(total, axis=-1, keepdims=True))
+    weights = terms / jnp.sum(terms, axis=-1, keepdims=True)
+    high = weights.astype(BF16).astype(F32)
+    both = jnp.concatenate([high, weights - high], axis=0).astype(BF16)
+    reads = []
+    for h in range(heads_dev):
+        read = jnp.dot(both, vals[0, h], preferred_element_type=F32)
+        reads.append(read[h:h + 1] + read[heads_dev + h:heads_dev + h + 1])
+    read_out[0] = jnp.concatenate(reads, axis=0).astype(BF16)
+    for move in moves:
+        move.wait()
 
 
 def local(tokens, kv_down, rope_down, kv_gain, key_up, value_up, query_nope, query_rope):
@@ -252,16 +264,15 @@
     hops = max(tp_count - 1, 1)
     count = len(bounds) - 1
     dma = pltpu.SemaphoreType.DMA
-    key_cache, value_cache, rope_t, read_out = pl.pallas_call(
-        functools.partial(kernel, sp_count, tp_count, bounds, (key_width + rope_width) ** (-0.5)),
+    parts = pl.pallas_call(
+        functools.partial(kernel, sp_count, tp_count, heads_dev, bounds),
         out_shape=(
             jax.ShapeDtypeStruct((1, heads_dev, length, key_width), BF16),
             jax.ShapeDtypeStruct((1, heads_dev, length, key_width), BF16),
             jax.ShapeDtypeStruct((1, rope_width, length), BF16),
-            jax.ShapeDtypeStruct((1, heads_dev, key_width), BF16),
         ),
-        in_specs=[any_space] * 10,
-        out_specs=(vmem,) * 4,
+        in_specs=[any_space] * 7,
+        out_specs=(vmem,) * 3,
         scratch_shapes=[
             pltpu.VMEM((sp_count + prompts, rows, latent_width), BF16),
             pltpu.VMEM(tokens.shape, BF16),
@@ -272,24 +283,29 @@
             pltpu.VMEM((latent_width * tile, key_width), F32),
             pltpu.VMEM((latent_width, heads_dev * key_width), BF16),
             pltpu.VMEM((latent_width, heads_dev * key_width), BF16),
-            pltpu.VMEM(query_nope.shape, BF16),
-            pltpu.VMEM(query_rope.shape, BF16),
             pltpu.VMEM((2, rope_width // 2, pos_dev), F32),
-            pltpu.VMEM((2, rope_width), F32),
-            pltpu.VMEM((heads_dev, length), F32),
-            dma((10,)),
+            dma((7,)),
             dma((2, hops, seq_local, count)),
             dma((2, hops, seq_local, count)),
             dma((prompts, count)),
             dma((sp_count, count)),
         ],
         compiler_params=pltpu.CompilerParams(
-            collective_id=0, has_side_effects=True, vmem_limit_bytes=40 * 1024 * 1024
+            collective_id=0, has_side_effects=True, vmem_limit_bytes=53000000
         ),
     )(
         tokens, kv_down, rope_down.T, kv_gain.reshape(1, latent_width), key_up, value_up,
-        query_nope, query_rope, jnp.asarray(cached), jnp.asarray(asked),
+        jnp.asarray(cached),
     )
+    key_cache, value_cache, rope_t, read_out = pl.pallas_call(
+        functools.partial(finish, (key_width + rope_width) ** (-0.5)),
+        out_shape=tuple(jax.ShapeDtypeStruct(part.shape, BF16) for part in parts)
+        + (jax.ShapeDtypeStruct((1, heads_dev, key_width), BF16),),
+        in_specs=[vmem] * 6,
+        out_specs=(any_space,) * 3 + (vmem,),
+        scratch_shapes=[dma((3,))],
+        compiler_params=pltpu.CompilerParams(vmem_limit_bytes=8 * 1024 * 1024),
+    )(*parts, query_nope, query_rope, jnp.asarray(asked))
     return (key_cache, value_cache, jnp.swapaxes(rope_t, 1, 2), read_out)
 
 

time: 44.6 us -> 35.3 us (0.79)
  local copies, waits for them, and re-layouts: 13.8 us -> 2.58 us
  Pallas kernels: 29.8 us -> 31.9 us
    unnamed x24 -> x12, local copies, waits for them, and re-layouts: 13.8 us -> 2.58 us
    pallas_call x1 -> x2, Pallas kernels: 29.8 us -> 31.9 us  [the longest x1 29.7 us: local(): pl.pallas_call(functools.partial(kernel, sp_count, tp_count, heads_dev, b...]
where the time goes in v2:
time: 35.3 us; the launch traced here: 35.1 us
  Pallas kernels  31.9 us (90%)
  local copies, waits for them, and re-layouts  2.58 us (7%)
  between operations  0.68 us (2%)
    pallas_call x1, Pallas kernels, local(): pl.pallas_call(functools.partial(kernel, sp_count, tp_count, heads_dev, b...  29.7 us
    unnamed x12, local copies, waits for them, and re-layouts  2.58 us
    pallas_call x1, Pallas kernels, local(): pl.pallas_call(functools.partial(finish, (key_width + rope_width) ** (-0....  2.17 us

profile of v2, /device:TPU:5, one launch (start us, length us, event | category | flops | bytes accessed | tf_op | source)
XLA Modules:
  0.0 35.1 jit_solution(16712335995729884157)
XLA Ops:
  0.6 0.0 copy-start
  0.6 0.9 %copy-done = bf16[2048,64]{0,1:T(8,128)(2,1)S(1)} copy-done((bf16[2048,64]{0,1:T(8,128)(2,1)S(1)}, bf16[2048,64]{0,1:T(8,128)(2,1)}, u32[]{:S(2)}) %copy-start) | copy-done | bytes 262168
  1.6 0.0 copy-start.1
  1.6 0.9 %copy-done.1 = f32[2,32,1024]{2,1,0:T(8,128)S(1)} copy-done((f32[2,32,1024]{2,1,0:T(8,128)S(1)}, f32[2,32,1024]{2,1,0:T(8,128)}, u32[]{:S(2)}) %copy-start.1) | copy-done | bytes 262168
  2.5 0.0 copy-start.2
  2.5 0.7 %copy-done.2 = f32[512]{0:T(512)S(1)} copy-done((f32[512]{0:T(512)S(1)}, f32[512]{0:T(512)}, u32[]{:S(2)}) %copy-start.2) | copy-done | bytes 2072
  3.2 0.0 copy-start.3
  3.2 0.0 copy-start.4
  3.2 0.0 copy-start.5
  3.2 29.7 %shard_map.129 = (bf16[1,4,1024,128]{3,2,1,0:T(8,128)(2,1)S(1)}, bf16[1,4,1024,128]{3,2,1,0:T(8,128)(2,1)S(1)}, bf16[1,64,1024]{2,1,0:T(8,128)(2,1)S(1)}) custom-call(bf16[1,256,2048]{2,1,0:T(8,128)(2,1)} %tok.1, bf16[2048,512]{1,0:T(8,128)(2,1)} %kvd.1, bf16[64,2048]{1,0:T(8,128)(2,1)S(1)} %bitcast.3, f32[1,512]{1,0:T(1,128)S(1)} %bitcast.4, ...), custom_call_target="tpu_custom_call" | custom-call | tf_op jit(solution)/shard_map/pallas_call | solution.py:267
  32.9 0.0 copy-done.3
  32.9 0.0 copy-done.4
  32.9 0.0 copy-done.5
  32.9 2.2 %shard_map.130 = (bf16[1,4,1024,128]{3,2,1,0:T(8,128)(2,1)}, bf16[1,4,1024,128]{3,2,1,0:T(8,128)(2,1)}, bf16[1,64,1024]{2,1,0:T(8,128)(2,1)}, bf16[1,4,128]{2,1,0:T(4,128)(2,1)}) custom-call(bf16[1,4,1024,128]{3,2,1,0:T(8,128)(2,1)S(1)} %get-tuple-element.11.keys, bf16[1,4,1024,128]{3,2,1,0:T(8,128)(2,1)S(1)} %get-tuple-element.12.vals, ...), custom_call_target="tpu_custom_call" | custom-call | tf_op jit(solution)/shard_map/pallas_call | solution.py:300
Async XLA Ops:
  0.6 1.0 %copy-start = (bf16[2048,64]{0,1:T(8,128)(2,1)S(1)}, bf16[2048,64]{0,1:T(8,128)(2,1)}, u32[]{:S(2)}) copy-start(bf16[2048,64]{0,1:T(8,128)(2,1)} %param.12) | copy-start | bytes 786436
  1.6 0.9 %copy-start.1 = (f32[2,32,1024]{2,1,0:T(8,128)S(1)}, f32[2,32,1024]{2,1,0:T(8,128)}, u32[]{:S(2)}) copy-start(f32[2,32,1024]{2,1,0:T(8,128)} %constant.4.clone.tab) | copy-start | bytes 786436
  2.5 0.7 %copy-start.2 = (f32[512]{0:T(512)S(1)}, f32[512]{0:T(512)}, u32[]{:S(2)}) copy-start(f32[512]{0:T(512)} %param.13) | copy-start | bytes 6148
  3.2 29.7 %copy-start.3 = (bf16[1,4,128]{2,1,0:T(4,128)(2,1)S(1)}, bf16[1,4,128]{2,1,0:T(4,128)(2,1)}, u32[]{:S(2)}) copy-start(bf16[1,4,128]{2,1,0:T(4,128)(2,1)} %query.1) | copy-start | bytes 3076
  3.2 29.7 %copy-start.4 = (bf16[1,4,64]{2,1,0:T(4,128)(2,1)S(1)}, bf16[1,4,64]{2,1,0:T(4,128)(2,1)}, u32[]{:S(2)}) copy-start(bf16[1,4,64]{2,1,0:T(4,128)(2,1)} %ask.1) | copy-start | bytes 1540
  3.2 29.7 %copy-start.5 = (f32[2,64]{1,0:T(2,128)S(1)}, f32[2,64]{1,0:T(2,128)}, u32[]{:S(2)}) copy-start(f32[2,64]{1,0:T(2,128)} %constant.5.clone.qtab) | copy-start | bytes 1540
